TPU v7x, 32 devices: a whole 2x2x4 slice. The times are simulated.
32 devices in a mesh: fs: 16 (over z, y, x), tp: 2 (over core).
Axes of the slice: x: 2, y: 2, z: 4, core: 2. Of those that a mesh axis runs over, the one named last changes fastest.
Arguments:
- tokens: bfloat16 [12288, 2048], P('fs'), may hold values from -6 to 6
- norm_gain: float32 [2048], replicated, may hold values from 0.1 to 1.9
- gate_weight: bfloat16 [2048, 5120], P('fs', 'tp'), may hold values from -0.125 to 0.125
- up_weight: bfloat16 [2048, 5120], P('fs', 'tp'), may hold values from -0.125 to 0.125
- down_weight: bfloat16 [5120, 2048], P('tp', 'fs'), may hold values from -0.078125 to 0.078125
Outputs:
- mixed: bfloat16 [12288, 2048], P(('fs', 'tp'))
All inputs are finite; a program needn't handle non-finite values.
Results may differ from a plain program's by a relative error of at most 0.014.
Values may be sent and summed in bfloat16 or wider, within the bound.
A program may use at most 128 MiB of HBM per device.

v0:
```python
import jax
import jax.numpy as jnp
from jax import lax
from jax.sharding import PartitionSpec as P


def add_rows(normed, piece):
    return jnp.dot(normed, piece, preferred_element_type=jnp.float32)


def per_device(tokens, norm_gain, gate_weight, up_weight, down_weight):
    values = tokens.astype(jnp.float32)
    scale = lax.rsqrt(jnp.mean(values * values, axis=-1, keepdims=True) + 1e-06)
    normed = (values * scale * norm_gain).astype(jnp.bfloat16)

    def add_single(piece):
        return add_rows(normed, piece)

    gate_proj = add_single(lax.all_gather(gate_weight, "fs", axis=0, tiled=True))
    up_proj = add_single(lax.all_gather(up_weight, "fs", axis=0, tiled=True))
    hidden = (jax.nn.silu(gate_proj) * up_proj).astype(jnp.bfloat16)
    down_whole = lax.all_gather(down_weight, "fs", axis=1, tiled=True)
    return lax.psum_scatter(
        jnp.dot(hidden, down_whole, preferred_element_type=jnp.float32).astype(jnp.bfloat16),
        "tp",
        scatter_dimension=0,
        tiled=True,
    )


def solution(mesh):
    in_specs = (P("fs", None), P(), P("fs", "tp"), P("fs", "tp"), P("tp", "fs"))
    out_specs = P(("fs", "tp"), None)
    return jax.shard_map(
        per_device, mesh=mesh, in_specs=in_specs, out_specs=out_specs, check_vma=False
    )
```

profile of v0, /device:TPU:0, one launch (start us, length us, event | category | flops | bytes accessed | tf_op | source)
XLA Modules:
  0.0 489.8 jit_solution(3628427633222220995)
XLA Ops:
  6.5 0.0 all-gather.4.cloned.1.call-start
  6.5 0.7 all-gather.4.cloned.1.call-update
  7.3 0.0 all-gather.6.cloned.1.call-start
  7.3 0.7 all-gather.6.cloned.1.call-update
  8.0 0.0 all-gather.8.cloned.1.call-start
  8.1 0.7 all-gather.8.cloned.1.call-update
  8.7 0.0 reduce-scatter.2.cloned.1.call-start
  8.8 2.6 fusion
  11.4 0.0 copy-start
  11.4 0.0 copy-start.1
  11.4 132.8 %all-gather.4.cloned.1.call-done = bf16[2048,2560]{1,0:T(8,128)(2,1)} async-done(((bf16[128,2560]{1,0:T(8,128)(2,1)}), bf16[2048,2560]{1,0:T(8,128)(2,1)}) %all-gather.4.cloned.1.call-update) | async-done | bytes 10485776 | tf_op jit(solution)/shard_map/all_gather | solution.py:19
  144.2 13.9 %fusion.5 = f32[768,2560]{1,0:T(8,128)} fusion(bf16[2048,2560]{1,0:T(8,128)(2,1)} %all-gather.4.cloned.1.call-done, bf16[768,2048]{1,0:T(8,128)(2,1)} %param.5, f32[2048]{0:T(1024)} %param.6, f32[768]{0:T(1024)S(1)} %add_rsqrt_fusion), kind=kOutput, calls=%fused_computation.7 | convolution fusion | flops 8059355136 | bytes 21507072 | tf_op jit(solution)/shard_map/dot_general | solution.py:8
  158.2 118.4 %all-gather.6.cloned.1.call-done = bf16[2048,2560]{1,0:T(8,128)(2,1)} async-done(((bf16[128,2560]{1,0:T(8,128)(2,1)}), bf16[2048,2560]{1,0:T(8,128)(2,1)}) %all-gather.6.cloned.1.call-update) | async-done | bytes 10485776 | tf_op jit(solution)/shard_map/all_gather | solution.py:20
  276.6 169.6 %all-gather.8.cloned.1.call-done = bf16[2560,2048]{1,0:T(8,128)(2,1)} async-done(((bf16[2560,128]{1,0:T(8,128)(2,1)}), bf16[2560,2048]{1,0:T(8,128)(2,1)}) %all-gather.8.cloned.1.call-update) | async-done | bytes 10485776 | tf_op jit(solution)/shard_map/all_gather | solution.py:22
  446.2 0.0 copy-done
  446.2 0.0 copy-done.1
  446.2 27.6 %convolution_convert_fusion = bf16[768,2048]{1,0:T(8,128)(2,1)} fusion(bf16[2560,2048]{1,0:T(8,128)(2,1)} %all-gather.8.cloned.1.call-done, f32[768,2560]{1,0:T(8,128)} %fusion.5, bf16[2048,2560]{1,0:T(8,128)(2,1)} %all-gather.6.cloned.1.call-done, bf16[768,2048]{1,0:T(8,128)(2,1)S(1)} %copy-done, f32[2048]{0:T(1024)S(1)} %copy-done.1, ...), kind=kOutput, calls=%fused_computation.6 | convolution fusion | flops 16125788160 | bytes 35138560 | tf_op jit(solution)/shard_map/dot_general | solution.py:24
  473.8 0.0 reduce-scatter.2.cloned.1.call-update
  473.8 9.5 %reduce-scatter.2.cloned.1.call-done = bf16[384,2048]{1,0:T(8,128)(2,1)} async-done(((bf16[768,2048]{1,0:T(8,128)(2,1)}), bf16[384,2048]{1,0:T(8,128)(2,1)}) %reduce-scatter.2.cloned.1.call-update) | async-done | bytes 1572880 | tf_op jit(solution)/shard_map/reduce_scatter | solution.py:23
  (1 shorter events, 0.0 us)
Async XLA Ops:
  6.5 137.7 %all-gather.4.cloned.1.call-start = ((), (), s32[]{:S(2)}) async-start(), calls=%async_computation.1 | async-start | bytes 11141120 | tf_op jit(solution)/shard_map/all_gather | solution.py:19
  7.3 269.4 %all-gather.6.cloned.1.call-start = ((), (), s32[]{:S(2)}) async-start(), calls=%async_computation.2 | async-start | bytes 11141120 | tf_op jit(solution)/shard_map/all_gather | solution.py:20
  8.0 438.2 %all-gather.8.cloned.1.call-start = ((), (), s32[]{:S(2)}) async-start(), calls=%async_computation.3 | async-start | bytes 11141120 | tf_op jit(solution)/shard_map/all_gather | solution.py:22
  8.7 474.6 %reduce-scatter.2.cloned.1.call-start = ((), (), s32[]{:S(2)}) async-start(), calls=%async_computation.4 | async-start | bytes 4718592 | tf_op jit(solution)/shard_map/reduce_scatter | solution.py:23
  11.4 434.8 %copy-start = (bf16[768,2048]{1,0:T(8,128)(2,1)S(1)}, bf16[768,2048]{1,0:T(8,128)(2,1)}, u32[]{:S(2)}) copy-start(bf16[768,2048]{1,0:T(8,128)(2,1)} %param.5) | copy-start | bytes 9437188
  11.4 434.8 %copy-start.1 = (f32[2048]{0:T(1024)S(1)}, f32[2048]{0:T(1024)}, u32[]{:S(2)}) copy-start(f32[2048]{0:T(1024)} %param.6) | copy-start | bytes 24580
Sparse Core Ops, SparseCore 0:
  10.0 134.1 all-gather.3
  146.9 129.6 all-gather.5
  279.3 166.8 all-gather.7
  473.9 9.3 reduce-scatter.1
where the time goes:
time: 490 us
  waiting for transfers between devices  432 us (88%)
  matrix products  41.5 us (8%)
  between operations  13.1 us (3%)
    all_gather x1, waiting for transfers between devices, per_device(): down_whole = lax.all_gather(down_weight, 'fs', axis=1, tiled=True)  170 us
    all_gather x1, waiting for transfers between devices, per_device(): lax.all_gather(gate_weight, 'fs', axis=0, tiled=True)  133 us
    all_gather x1, waiting for transfers between devices, per_device(): up_proj = add_single(lax.all_gather(up_weight, 'fs', axis=0, tiled=True))  118 us
    dot_general x1, matrix products, per_device(): jnp.dot(hidden, down_whole, preferred_element_type=jnp.float32)  27.6 us
    dot_general x1, matrix products, add_rows(): return jnp.dot(normed, piece, preferred_element_type=jnp.float32)  13.9 us
  transfers between devices with their start and end apart: 4, of which 4 were waited for; matrix products, arithmetic and copies ran while one was open for 3% of the time, Pallas kernels for 0%

commit v1 on v0

--- a/solution.py
+++ b/solution.py
@@ -2,6 +2,21 @@
 import jax.numpy as jnp
 from jax import lax
 from jax.sharding import PartitionSpec as P
+from jax.lax import axis_index, ppermute, psum
+
+
+def move_fields(x_local):
+    devs = psum(1, "fs")
+    o_now = [(i0 - 1, i0) for i0 in range(1, devs)] + [(devs - 1, 0)]
+    tmp = x_local
+    b = 0
+    slots = [tmp]
+    while b < devs - 1:
+        tmp = ppermute(tmp, "fs", o_now)
+        slots += [tmp]
+        b += 1
+    mid_arr = jnp.concatenate([*reversed(slots)], axis=1)
+    return jnp.roll(mid_arr, (axis_index("fs") + 1) * tmp.shape[1], axis=1)
 
 
 def add_rows(normed, piece):
@@ -19,7 +34,7 @@
     gate_proj = add_single(lax.all_gather(gate_weight, "fs", axis=0, tiled=True))
     up_proj = add_single(lax.all_gather(up_weight, "fs", axis=0, tiled=True))
     hidden = (jax.nn.silu(gate_proj) * up_proj).astype(jnp.bfloat16)
-    down_whole = lax.all_gather(down_weight, "fs", axis=1, tiled=True)
+    down_whole = move_fields(down_weight)
     return lax.psum_scatter(
         jnp.dot(hidden, down_whole, preferred_element_type=jnp.float32).astype(jnp.bfloat16),
         "tp",

time: 490 us -> 553 us (1.13)
  local copies, waits for them, and re-layouts: 0.01 us -> 56.7 us
    ppermute x0 -> x15, waiting for transfers between devices: none -> 412 us  [move_fields(): tmp = ppermute(tmp, 'fs', o_now)]
    all_gather x1 -> x0, waiting for transfers between devices: 170 us -> none  [per_device(): down_whole = lax.all_gather(down_weight, 'fs', axis=1, tiled=True)]
    all_gather x1, waiting for transfers between devices: 133 us -> 0.01 us  [per_device(): lax.all_gather(gate_weight, 'fs', axis=0, tiled=True)]
    all_gather x1, waiting for transfers between devices: 118 us -> 0.01 us  [per_device(): up_proj = add_single(lax.all_gather(up_weight, 'fs', axis=0, tiled=True))]
    unnamed x4 -> x89, local copies, waits for them, and re-layouts: 0.01 us -> 55.8 us
    dot_general x1, matrix products: 27.6 us -> 12.3 us  [per_device(): jnp.dot(hidden, down_whole, preferred_element_type=jnp.float32)]
    reduce_scatter x1, waiting for transfers between devices: 9.51 us -> 24.1 us  [per_device(): lax.psum_scatter(jnp.dot(hidden, down_whole, preferred_element_type=jnp.f...]
    dot_general x1 -> x2, matrix products: 13.9 us -> 26.8 us  [add_rows(): return jnp.dot(normed, piece, preferred_element_type=jnp.float32)]
  transfers between devices with their start and end apart: 4 -> 18, of which waited for: 4 -> 16; matrix products, arithmetic and copies ran while one was open for 3% -> 11% of each run, Pallas kernels for 0% -> 0%
where the time goes in v1:
time: 553 us; the launch traced here: 552 us
  waiting for transfers between devices  437 us (79%)
  local copies, waits for them, and re-layouts  56.7 us (10%)
  matrix products  39.1 us (7%)
  between operations  13.3 us (2%)
    ppermute x15, waiting for transfers between devices, move_fields(): tmp = ppermute(tmp, 'fs', o_now)  412 us
    unnamed x89, local copies, waits for them, and re-layouts  55.8 us
    dot_general x2, matrix products, add_rows(): return jnp.dot(normed, piece, preferred_element_type=jnp.float32)  26.8 us
    reduce_scatter x1, waiting for transfers between devices, per_device(): lax.psum_scatter(jnp.dot(hidden, down_whole, preferred_element_type=jnp.f...  24.1 us
    dot_general x1, matrix products, per_device(): jnp.dot(hidden, down_whole, preferred_element_type=jnp.float32)  12.3 us
  transfers between devices with their start and end apart: 18, of which 16 were waited for; matrix products, arithmetic and copies ran while one was open for 11% of the time, Pallas kernels for 0%

profile of v1, /device:TPU:0, one launch (start us, length us, event | category | flops | bytes accessed | tf_op | source)
XLA Modules:
  0.0 552.4 jit_solution(17626052501318226953)
XLA Ops:
  7.3 3.0 collective-permute-start
  10.3 20.8 %collective-permute-done = bf16[2560,128]{1,0:T(8,128)(2,1)S(1)} collective-permute-done((bf16[2560,128]{1,0:T(8,128)(2,1)}, bf16[2560,128]{1,0:T(8,128)(2,1)S(1)}, u32[]{:S(2)}, u32[]{:S(2)}) %collective-permute-start) | collective-permute-done | bytes 655392 | tf_op jit(solution)/shard_map/ppermute | solution.py:15
  32.0 25.5 %collective-permute-done.1 = bf16[2560,128]{1,0:T(8,128)(2,1)S(1)} collective-permute-done((bf16[2560,128]{1,0:T(8,128)(2,1)S(1)}, bf16[2560,128]{1,0:T(8,128)(2,1)S(1)}, u32[]{:S(2)}, u32[]{:S(2)}) %collective-permute-start.1) | collective-permute-done | bytes 655392 | tf_op jit(solution)/shard_map/ppermute | solution.py:15
  58.4 32.1 %collective-permute-done.2 = bf16[2560,128]{1,0:T(8,128)(2,1)S(1)} collective-permute-done((bf16[2560,128]{1,0:T(8,128)(2,1)S(1)}, bf16[2560,128]{1,0:T(8,128)(2,1)S(1)}, u32[]{:S(2)}, u32[]{:S(2)}) %collective-permute-start.2) | collective-permute-done | bytes 655392 | tf_op jit(solution)/shard_map/ppermute | solution.py:15
  91.3 25.6 %collective-permute-done.3 = bf16[2560,128]{1,0:T(8,128)(2,1)S(1)} collective-permute-done((bf16[2560,128]{1,0:T(8,128)(2,1)S(1)}, bf16[2560,128]{1,0:T(8,128)(2,1)S(1)}, u32[]{:S(2)}, u32[]{:S(2)}) %collective-permute-start.3) | collective-permute-done | bytes 655392 | tf_op jit(solution)/shard_map/ppermute | solution.py:15
  117.7 34.3 %collective-permute-done.4 = bf16[2560,128]{1,0:T(8,128)(2,1)S(1)} collective-permute-done((bf16[2560,128]{1,0:T(8,128)(2,1)S(1)}, bf16[2560,128]{1,0:T(8,128)(2,1)S(1)}, u32[]{:S(2)}, u32[]{:S(2)}) %collective-permute-start.4) | collective-permute-done | bytes 655392 | tf_op jit(solution)/shard_map/ppermute | solution.py:15
  152.1 29.4 %collective-permute-done.5 = bf16[2560,128]{1,0:T(8,128)(2,1)S(1)} collective-permute-done((bf16[2560,128]{1,0:T(8,128)(2,1)S(1)}, bf16[2560,128]{1,0:T(8,128)(2,1)S(1)}, u32[]{:S(2)}, u32[]{:S(2)}) %collective-permute-start.5) | collective-permute-done | bytes 655392 | tf_op jit(solution)/shard_map/ppermute | solution.py:15
  181.5 32.6 %collective-permute-done.6 = bf16[2560,128]{1,0:T(8,128)(2,1)S(1)} collective-permute-done((bf16[2560,128]{1,0:T(8,128)(2,1)S(1)}, bf16[2560,128]{1,0:T(8,128)(2,1)S(1)}, u32[]{:S(2)}, u32[]{:S(2)}) %collective-permute-start.6) | collective-permute-done | bytes 655392 | tf_op jit(solution)/shard_map/ppermute | solution.py:15
  214.9 26.8 %collective-permute-done.7 = bf16[2560,128]{1,0:T(8,128)(2,1)S(1)} collective-permute-done((bf16[2560,128]{1,0:T(8,128)(2,1)S(1)}, bf16[2560,128]{1,0:T(8,128)(2,1)S(1)}, u32[]{:S(2)}, u32[]{:S(2)}) %collective-permute-start.7) | collective-permute-done | bytes 655392 | tf_op jit(solution)/shard_map/ppermute | solution.py:15
  242.6 24.0 %collective-permute-done.8 = bf16[2560,128]{1,0:T(8,128)(2,1)S(1)} collective-permute-done((bf16[2560,128]{1,0:T(8,128)(2,1)S(1)}, bf16[2560,128]{1,0:T(8,128)(2,1)S(1)}, u32[]{:S(2)}, u32[]{:S(2)}) %collective-permute-start.8) | collective-permute-done | bytes 655392 | tf_op jit(solution)/shard_map/ppermute | solution.py:15
  267.5 31.5 %collective-permute-done.9 = bf16[2560,128]{1,0:T(8,128)(2,1)S(1)} collective-permute-done((bf16[2560,128]{1,0:T(8,128)(2,1)S(1)}, bf16[2560,128]{1,0:T(8,128)(2,1)S(1)}, u32[]{:S(2)}, u32[]{:S(2)}) %collective-permute-start.9) | collective-permute-done | bytes 655392 | tf_op jit(solution)/shard_map/ppermute | solution.py:15
  299.8 22.3 %collective-permute-done.10 = bf16[2560,128]{1,0:T(8,128)(2,1)S(1)} collective-permute-done((bf16[2560,128]{1,0:T(8,128)(2,1)S(1)}, bf16[2560,128]{1,0:T(8,128)(2,1)S(1)}, u32[]{:S(2)}, u32[]{:S(2)}) %collective-permute-start.10) | collective-permute-done | bytes 655392 | tf_op jit(solution)/shard_map/ppermute | solution.py:15
  323.0 33.0 %collective-permute-done.11 = bf16[2560,128]{1,0:T(8,128)(2,1)S(1)} collective-permute-done((bf16[2560,128]{1,0:T(8,128)(2,1)S(1)}, bf16[2560,128]{1,0:T(8,128)(2,1)S(1)}, u32[]{:S(2)}, u32[]{:S(2)}) %collective-permute-start.11) | collective-permute-done | bytes 655392 | tf_op jit(solution)/shard_map/ppermute | solution.py:15
  356.9 32.9 %collective-permute-done.12 = bf16[2560,128]{1,0:T(8,128)(2,1)S(1)} collective-permute-done((bf16[2560,128]{1,0:T(8,128)(2,1)S(1)}, bf16[2560,128]{1,0:T(8,128)(2,1)S(1)}, u32[]{:S(2)}, u32[]{:S(2)}) %collective-permute-start.12) | collective-permute-done | bytes 655392 | tf_op jit(solution)/shard_map/ppermute | solution.py:15
  390.6 26.7 %collective-permute-done.13 = bf16[2560,128]{1,0:T(8,128)(2,1)} collective-permute-done((bf16[2560,128]{1,0:T(8,128)(2,1)S(1)}, bf16[2560,128]{1,0:T(8,128)(2,1)}, u32[]{:S(2)}, u32[]{:S(2)}) %collective-permute-start.13) | collective-permute-done | bytes 655392 | tf_op jit(solution)/shard_map/ppermute | solution.py:15
  417.4 2.7 fusion.2
  420.2 15.0 %collective-permute-done.14 = bf16[2560,128]{1,0:T(8,128)(2,1)} collective-permute-done((bf16[2560,128]{1,0:T(8,128)(2,1)}, bf16[2560,128]{1,0:T(8,128)(2,1)}, u32[]{:S(2)}, u32[]{:S(2)}) %collective-permute-start.14) | collective-permute-done | bytes 655392 | tf_op jit(solution)/shard_map/ppermute | solution.py:15
  435.2 2.1 constant_dynamic-update-slice_fusion.31
  441.3 2.0 constant_dynamic-update-slice_fusion.28
  467.4 2.1 constant_dynamic-update-slice_fusion.14
  482.6 13.0 %fusion.9 = f32[768,2560]{1,0:T(8,128)} fusion(bf16[2048,2560]{1,0:T(8,128)(2,1)} %all-gather.3.cloned.1.call-done, bf16[768,2048]{1,0:T(8,128)(2,1)S(1)} %copy-done, f32[2048]{0:T(1024)S(1)} %copy-done.28, f32[768]{0:T(1024)S(1)} %add_rsqrt_fusion), kind=kOutput, calls=%fused_computation.9 | convolution fusion | flops 8059355136 | bytes 21507072 | tf_op jit(solution)/shard_map/dot_general | solution.py:23
  495.6 13.9 %multiply_convert_fusion = bf16[768,2560]{1,0:T(8,128)(2,1)S(1)} fusion(f32[768,2560]{1,0:T(8,128)} %fusion.9, bf16[2048,2560]{1,0:T(8,128)(2,1)} %all-gather.5.cloned.1.call-done, bf16[768,2048]{1,0:T(8,128)(2,1)S(1)} %copy-done, f32[2048]{0:T(1024)S(1)} %copy-done.28, f32[768]{0:T(1024)S(1)} %add_rsqrt_fusion), kind=kOutput, calls=%fused_computation.2 | convolution fusion | flops 8071151616 | bytes 25439232 | tf_op jit(solution)/shard_map/dot_general | solution.py:23
  509.4 12.3 %fusion.5 = bf16[768,2048]{1,0:T(8,128)(2,1)} fusion(bf16[768,2560]{1,0:T(8,128)(2,1)S(1)} %multiply_convert_fusion, bf16[2560,4096]{1,0:T(8,128)(2,1)} %constant_dynamic-update-slice_fusion, s32[]{:T(128)S(6)} %select_n.14), kind=kOutput, calls=%fused_computation.8 | convolution fusion | flops 8054636544 | bytes 17563652 | tf_op jit(solution)/shard_map/dot_general | solution.py:39
  521.7 24.1 %reduce-scatter.2.cloned.1.call-done = bf16[384,2048]{1,0:T(8,128)(2,1)} async-done(((bf16[768,2048]{1,0:T(8,128)(2,1)}), bf16[384,2048]{1,0:T(8,128)(2,1)}) %reduce-scatter.2.cloned.1.call-update) | async-done | bytes 1572880 | tf_op jit(solution)/shard_map/reduce_scatter | solution.py:38
  (110 shorter events, 51.4 us)
Async XLA Ops:
  6.5 476.0 %all-gather.3.cloned.1.call-start = ((), (), s32[]{:S(2)}) async-start(), calls=%async_computation.1 | async-start | bytes 11141120 | tf_op jit(solution)/shard_map/all_gather | solution.py:34
  7.3 488.3 %all-gather.5.cloned.1.call-start = ((), (), s32[]{:S(2)}) async-start(), calls=%async_computation.2 | async-start | bytes 11141120 | tf_op jit(solution)/shard_map/all_gather | solution.py:35
  7.3 23.8 %collective-permute-start = (bf16[2560,128]{1,0:T(8,128)(2,1)}, bf16[2560,128]{1,0:T(8,128)(2,1)S(1)}, u32[]{:S(2)}, u32[]{:S(2)}) collective-permute-start(bf16[2560,128]{1,0:T(8,128)(2,1)} %param.9), channel_id=1, source_target_pairs={{0,2},{2,4},{4,6},{6,8},{8,10},{10,12},{12,14},{14,16},{16,18},{18... | collective-permute-start | bytes 1966088 | tf_op jit(solution)/shard_map/ppermute | solution.py:15
  32.0 25.5 %collective-permute-start.1 = (bf16[2560,128]{1,0:T(8,128)(2,1)S(1)}, bf16[2560,128]{1,0:T(8,128)(2,1)S(1)}, u32[]{:S(2)}, u32[]{:S(2)}) collective-permute-start(bf16[2560,128]{1,0:T(8,128)(2,1)S(1)} %collective-permute-done), channel_id=1, source_target_pairs={{0,2},{2,4},{4,6},{6,8},{8,10},{10,12},{12,14},{14,16},{16,18},{18... | collective-permute-start | bytes 1966088 | tf_op jit(solution)/shard_map/ppermute | solution.py:15
  58.3 32.1 %collective-permute-start.2 = (bf16[2560,128]{1,0:T(8,128)(2,1)S(1)}, bf16[2560,128]{1,0:T(8,128)(2,1)S(1)}, u32[]{:S(2)}, u32[]{:S(2)}) collective-permute-start(bf16[2560,128]{1,0:T(8,128)(2,1)S(1)} %collective-permute-done.1), channel_id=1, source_target_pairs={{0,2},{2,4},{4,6},{6,8},{8,10},{10,12},{12,14},{14,16},{16,18},{18... | collective-permute-start | bytes 1966088 | tf_op jit(solution)/shard_map/ppermute | solution.py:15
  91.3 25.6 %collective-permute-start.3 = (bf16[2560,128]{1,0:T(8,128)(2,1)S(1)}, bf16[2560,128]{1,0:T(8,128)(2,1)S(1)}, u32[]{:S(2)}, u32[]{:S(2)}) collective-permute-start(bf16[2560,128]{1,0:T(8,128)(2,1)S(1)} %collective-permute-done.2), channel_id=1, source_target_pairs={{0,2},{2,4},{4,6},{6,8},{8,10},{10,12},{12,14},{14,16},{16,18},{18... | collective-permute-start | bytes 1966088 | tf_op jit(solution)/shard_map/ppermute | solution.py:15
  117.7 34.3 %collective-permute-start.4 = (bf16[2560,128]{1,0:T(8,128)(2,1)S(1)}, bf16[2560,128]{1,0:T(8,128)(2,1)S(1)}, u32[]{:S(2)}, u32[]{:S(2)}) collective-permute-start(bf16[2560,128]{1,0:T(8,128)(2,1)S(1)} %collective-permute-done.3), channel_id=1, source_target_pairs={{0,2},{2,4},{4,6},{6,8},{8,10},{10,12},{12,14},{14,16},{16,18},{18... | collective-permute-start | bytes 1966088 | tf_op jit(solution)/shard_map/ppermute | solution.py:15
  152.0 268.1 %copy-start.10 = (bf16[2560,128]{1,0:T(8,128)(2,1)}, bf16[2560,128]{1,0:T(8,128)(2,1)S(1)}, u32[]{:S(2)}) copy-start(bf16[2560,128]{1,0:T(8,128)(2,1)S(1)} %collective-permute-done.4) | copy-start | bytes 1966084
  152.0 29.5 %collective-permute-start.5 = (bf16[2560,128]{1,0:T(8,128)(2,1)S(1)}, bf16[2560,128]{1,0:T(8,128)(2,1)S(1)}, u32[]{:S(2)}, u32[]{:S(2)}) collective-permute-start(bf16[2560,128]{1,0:T(8,128)(2,1)S(1)} %collective-permute-done.4), channel_id=1, source_target_pairs={{0,2},{2,4},{4,6},{6,8},{8,10},{10,12},{12,14},{14,16},{16,18},{18... | collective-permute-start | bytes 1966088 | tf_op jit(solution)/shard_map/ppermute | solution.py:15
  152.1 393.8 %reduce-scatter.2.cloned.1.call-start = ((), (), s32[]{:S(2)}) async-start(), calls=%async_computation.3 | async-start | bytes 4718592 | tf_op jit(solution)/shard_map/reduce_scatter | solution.py:38
  181.5 238.6 %copy-start.12 = (bf16[2560,128]{1,0:T(8,128)(2,1)}, bf16[2560,128]{1,0:T(8,128)(2,1)S(1)}, u32[]{:S(2)}) copy-start(bf16[2560,128]{1,0:T(8,128)(2,1)S(1)} %collective-permute-done.5) | copy-start | bytes 1966084
  181.5 32.6 %collective-permute-start.6 = (bf16[2560,128]{1,0:T(8,128)(2,1)S(1)}, bf16[2560,128]{1,0:T(8,128)(2,1)S(1)}, u32[]{:S(2)}, u32[]{:S(2)}) collective-permute-start(bf16[2560,128]{1,0:T(8,128)(2,1)S(1)} %collective-permute-done.5), channel_id=1, source_target_pairs={{0,2},{2,4},{4,6},{6,8},{8,10},{10,12},{12,14},{14,16},{16,18},{18... | collective-permute-start | bytes 1966088 | tf_op jit(solution)/shard_map/ppermute | solution.py:15
  214.9 26.8 %collective-permute-start.7 = (bf16[2560,128]{1,0:T(8,128)(2,1)S(1)}, bf16[2560,128]{1,0:T(8,128)(2,1)S(1)}, u32[]{:S(2)}, u32[]{:S(2)}) collective-permute-start(bf16[2560,128]{1,0:T(8,128)(2,1)S(1)} %collective-permute-done.6), channel_id=1, source_target_pairs={{0,2},{2,4},{4,6},{6,8},{8,10},{10,12},{12,14},{14,16},{16,18},{18... | collective-permute-start | bytes 1966088 | tf_op jit(solution)/shard_map/ppermute | solution.py:15
  242.5 24.0 %collective-permute-start.8 = (bf16[2560,128]{1,0:T(8,128)(2,1)S(1)}, bf16[2560,128]{1,0:T(8,128)(2,1)S(1)}, u32[]{:S(2)}, u32[]{:S(2)}) collective-permute-start(bf16[2560,128]{1,0:T(8,128)(2,1)S(1)} %collective-permute-done.7), channel_id=1, source_target_pairs={{0,2},{2,4},{4,6},{6,8},{8,10},{10,12},{12,14},{14,16},{16,18},{18... | collective-permute-start | bytes 1966088 | tf_op jit(solution)/shard_map/ppermute | solution.py:15
  267.5 31.5 %collective-permute-start.9 = (bf16[2560,128]{1,0:T(8,128)(2,1)S(1)}, bf16[2560,128]{1,0:T(8,128)(2,1)S(1)}, u32[]{:S(2)}, u32[]{:S(2)}) collective-permute-start(bf16[2560,128]{1,0:T(8,128)(2,1)S(1)} %collective-permute-done.8), channel_id=1, source_target_pairs={{0,2},{2,4},{4,6},{6,8},{8,10},{10,12},{12,14},{14,16},{16,18},{18... | collective-permute-start | bytes 1966088 | tf_op jit(solution)/shard_map/ppermute | solution.py:15
  299.8 22.3 %collective-permute-start.10 = (bf16[2560,128]{1,0:T(8,128)(2,1)S(1)}, bf16[2560,128]{1,0:T(8,128)(2,1)S(1)}, u32[]{:S(2)}, u32[]{:S(2)}) collective-permute-start(bf16[2560,128]{1,0:T(8,128)(2,1)S(1)} %collective-permute-done.9), channel_id=1, source_target_pairs={{0,2},{2,4},{4,6},{6,8},{8,10},{10,12},{12,14},{14,16},{16,18},{18... | collective-permute-start | bytes 1966088 | tf_op jit(solution)/shard_map/ppermute | solution.py:15
  323.0 33.0 %collective-permute-start.11 = (bf16[2560,128]{1,0:T(8,128)(2,1)S(1)}, bf16[2560,128]{1,0:T(8,128)(2,1)S(1)}, u32[]{:S(2)}, u32[]{:S(2)}) collective-permute-start(bf16[2560,128]{1,0:T(8,128)(2,1)S(1)} %collective-permute-done.10), channel_id=1, source_target_pairs={{0,2},{2,4},{4,6},{6,8},{8,10},{10,12},{12,14},{14,16},{16,18},{18... | collective-permute-start | bytes 1966088 | tf_op jit(solution)/shard_map/ppermute | solution.py:15
  356.9 32.9 %collective-permute-start.12 = (bf16[2560,128]{1,0:T(8,128)(2,1)S(1)}, bf16[2560,128]{1,0:T(8,128)(2,1)S(1)}, u32[]{:S(2)}, u32[]{:S(2)}) collective-permute-start(bf16[2560,128]{1,0:T(8,128)(2,1)S(1)} %collective-permute-done.11), channel_id=1, source_target_pairs={{0,2},{2,4},{4,6},{6,8},{8,10},{10,12},{12,14},{14,16},{16,18},{18... | collective-permute-start | bytes 1966088 | tf_op jit(solution)/shard_map/ppermute | solution.py:15
  390.6 26.7 %collective-permute-start.13 = (bf16[2560,128]{1,0:T(8,128)(2,1)S(1)}, bf16[2560,128]{1,0:T(8,128)(2,1)}, u32[]{:S(2)}, u32[]{:S(2)}) collective-permute-start(bf16[2560,128]{1,0:T(8,128)(2,1)S(1)} %collective-permute-done.12), channel_id=1, source_target_pairs={{0,2},{2,4},{4,6},{6,8},{8,10},{10,12},{12,14},{14,16},{16,18},{18... | collective-permute-start | bytes 1966088 | tf_op jit(solution)/shard_map/ppermute | solution.py:15
  417.3 17.9 %collective-permute-start.14 = (bf16[2560,128]{1,0:T(8,128)(2,1)}, bf16[2560,128]{1,0:T(8,128)(2,1)}, u32[]{:S(2)}, u32[]{:S(2)}) collective-permute-start(bf16[2560,128]{1,0:T(8,128)(2,1)} %collective-permute-done.13), channel_id=1, source_target_pairs={{0,2},{2,4},{4,6},{6,8},{8,10},{10,12},{12,14},{14,16},{16,18},{18... | collective-permute-start | bytes 1966088 | tf_op jit(solution)/shard_map/ppermute | solution.py:15
  417.3 61.5 %copy-start.7 = (bf16[2560,128]{1,0:T(8,128)(2,1)S(1)}, bf16[2560,128]{1,0:T(8,128)(2,1)}, u32[]{:S(2)}) copy-start(bf16[2560,128]{1,0:T(8,128)(2,1)} %copy-done.6) | copy-start | bytes 1966084
  417.4 62.4 %copy-start.5 = (bf16[2560,128]{1,0:T(8,128)(2,1)S(1)}, bf16[2560,128]{1,0:T(8,128)(2,1)}, u32[]{:S(2)}) copy-start(bf16[2560,128]{1,0:T(8,128)(2,1)} %copy-done.4) | copy-start | bytes 1966084
  420.1 62.4 %copy-start = (bf16[768,2048]{1,0:T(8,128)(2,1)S(1)}, bf16[768,2048]{1,0:T(8,128)(2,1)}, u32[]{:S(2)}) copy-start(bf16[768,2048]{1,0:T(8,128)(2,1)} %param.5) | copy-start | bytes 9437188
  420.1 62.4 %copy-start.28 = (f32[2048]{0:T(1024)S(1)}, f32[2048]{0:T(1024)}, u32[]{:S(2)}) copy-start(f32[2048]{0:T(1024)} %param.6) | copy-start | bytes 24580
  (23 other events, 660.8 us)
Sparse Core Ops, SparseCore 0:
  10.0 187.1 all-gather.2
  199.9 200.9 all-gather.4
  521.8 23.9 reduce-scatter.1
